TPU v7x, 32 devices: a whole 2x2x4 slice. The times are simulated.
32 devices in a mesh: sp: 16 (over z, y, core), tp: 2 (over x).
Axes of the slice: x: 2, y: 2, z: 4, core: 2. Of those that a mesh axis runs over, the one named last changes fastest.
Arguments:
- inputs: bfloat16 [2, 2048, 1024], P(None, 'sp'), may hold values from -6 to 6
- queries: bfloat16 [2, 2048, 4, 128], P(None, 'sp', 'tp'), may hold values from -6 to 6
- values: bfloat16 [2, 2048, 4, 256], P(None, 'sp', 'tp'), may hold values from -6 to 6
- out_grad: bfloat16 [2, 2048, 4, 256], P(None, 'sp', 'tp'), may hold values from -6 to 6
- key_weight: bfloat16 [1024, 4, 128], P(None, 'tp'), may hold values from -6 to 6
- decay_ahead: float32 [4], P('tp'), may hold values from -2.9 to 2.2
- decay_behind: float32 [4], P('tp'), may hold values from -2.9 to 2.2
Outputs:
- query_grad: bfloat16 [2, 2048, 4, 128], P(None, 'sp', 'tp')
- value_grad: bfloat16 [2, 2048, 4, 256], P(None, 'sp', 'tp')
- input_grad: bfloat16 [2, 2048, 1024], P('tp', 'sp')
- weight_grad: float32 [1024, 4, 128], P('sp', 'tp')
- decay_grad: float32 [2, 4], P(None, 'tp')
All inputs are finite; a program needn't handle non-finite values.
Results may differ from a plain program's by a relative error of at most 0.015.
Values may be sent and summed in bfloat16 or wider, within the bound.
A program may use at most 256 MiB of HBM per device.

v0:
```python
import math
import jax
import jax.numpy as jnp
from jax import lax
from jax.sharding import PartitionSpec as P

HIGHEST = lax.Precision.HIGHEST


def prefix(value, axis, join, neutral, backward):
    count, mine = (lax.axis_size(axis), lax.axis_index(axis))
    pieces = jax.tree.map(lambda part: lax.all_gather(part, axis), value)
    if backward:
        pieces = jax.tree.map(lambda part: part[::-1], pieces)
        mine = count - 1 - mine
    subtotal = jax.tree.map(
        lambda part, zero: jnp.full_like(part, 0) + jnp.asarray(zero, part.dtype), value, neutral
    )

    def step(position, subtotal):
        longer = join(subtotal, jax.tree.map(lambda part: part[position], pieces))
        return jax.tree.map(lambda new, old: jnp.where(position < mine, new, old), longer, subtotal)

    return lax.fori_loop(0, count - 1, step, subtotal)


def own_rows(contribution, rows, axis):
    whole = contribution(jnp.int32(0), rows * lax.axis_size(axis))
    return lax.psum_scatter(whole, axis, scatter_dimension=0, tiled=True)


def summed_rows(product, rows, axis):
    everything = product(jnp.int32(0), lax.axis_size(axis) * rows)
    own = lax.psum_scatter(everything.astype(jnp.bfloat16), axis, scatter_dimension=0, tiled=True)
    return own.astype(jnp.float32)


def link_states(earlier, later):
    return (
        earlier[0] * later[0],
        later[0] * earlier[1] + later[1],
        earlier[2] * later[2],
        later[2] * earlier[3] + later[3],
    )


def shards(inputs, queries, values, out_grad, key_weight, decay_ahead, decay_behind):
    batch_seqs, length, in_width = inputs.shape
    devices = lax.axis_size("sp")
    my_index = lax.axis_index("sp").astype(jnp.float32)
    all_tokens = length * devices
    key_scale = 1.0 / math.sqrt(in_width * queries.shape[3] * all_tokens)
    rate_ahead = jax.nn.log_sigmoid(decay_ahead) / all_tokens
    rate_behind = jax.nn.log_sigmoid(decay_behind) / all_tokens
    key_raw = jnp.einsum(
        "bld,dhk->blhk", inputs, key_weight, preferred_element_type=jnp.float32
    ).astype(jnp.bfloat16)
    keys = key_raw.astype(jnp.float32) * key_scale
    query_wide = queries.astype(jnp.float32)
    value_wide = values.astype(jnp.float32)
    grad_wide = out_grad.astype(jnp.float32)
    offsets = jnp.arange(length, dtype=jnp.float32)
    distance = offsets[:, None] - offsets[None, :]
    mask_ahead = jnp.where(
        distance[None] >= 0, jnp.exp(distance[None] * rate_ahead[:, None, None]), 0.0
    )
    mask_behind = jnp.where(
        distance[None] <= 0, jnp.exp(-distance[None] * rate_behind[:, None, None]), 0.0
    )
    mask_both = (mask_ahead + mask_behind)[None]
    keep_ahead = jnp.exp((length - 1.0 - offsets)[:, None] * rate_ahead[None])[None, :, :, None]
    keep_behind = jnp.exp(offsets[:, None] * rate_behind[None])[None, :, :, None]
    reach_ahead = jnp.exp((offsets + 1.0)[:, None] * rate_ahead[None])[None, :, :, None]
    reach_behind = jnp.exp((length - offsets)[:, None] * rate_behind[None])[None, :, :, None]
    scores = (
        jnp.einsum("bthk,bshk->bhts", queries, key_raw, preferred_element_type=jnp.float32)
        * key_scale
    )
    grad_scores = jnp.einsum(
        "bthv,bshv->bhts", out_grad, values, preferred_element_type=jnp.float32
    )
    sums_ahead = jnp.einsum("bshk,bshv->bhkv", keys * keep_ahead, value_wide, precision=HIGHEST)
    sums_behind = jnp.einsum("bshk,bshv->bhkv", keys * keep_behind, value_wide, precision=HIGHEST)
    pulls_ahead = jnp.einsum(
        "bthk,bthv->bhkv", query_wide * reach_ahead, grad_wide, precision=HIGHEST
    )
    pulls_behind = jnp.einsum(
        "bthk,bthv->bhkv", query_wide * reach_behind, grad_wide, precision=HIGHEST
    )
    span_ahead = jnp.exp(length * rate_ahead).reshape(1, -1, 1, 1)
    span_behind = jnp.exp(length * rate_behind).reshape(1, -1, 1, 1)
    unit_span = jnp.ones_like(span_ahead)
    zero_state = jnp.zeros_like(sums_ahead)
    upward = prefix(
        (span_ahead, sums_ahead, span_behind, pulls_behind),
        "sp",
        link_states,
        (unit_span, zero_state, unit_span, zero_state),
        False,
    )
    downward = prefix(
        (span_behind, sums_behind, span_ahead, pulls_ahead),
        "sp",
        link_states,
        (unit_span, zero_state, unit_span, zero_state),
        True,
    )
    state_ahead, pull_behind = (upward[1], upward[3])
    state_behind, pull_ahead = (downward[1], downward[3])
    out_ahead = jnp.einsum(
        "bhts,bshv->bthv", scores * mask_ahead[None], value_wide, precision=HIGHEST
    )
    out_ahead = out_ahead + jnp.einsum(
        "bthk,bhkv->bthv", query_wide * reach_ahead, state_ahead, precision=HIGHEST
    )
    out_behind = jnp.einsum(
        "bhts,bshv->bthv", scores * mask_behind[None], value_wide, precision=HIGHEST
    )
    out_behind = out_behind + jnp.einsum(
        "bthk,bhkv->bthv", query_wide * reach_behind, state_behind, precision=HIGHEST
    )
    grad_q = jnp.einsum("bhts,bshk->bthk", grad_scores * mask_both, keys, precision=HIGHEST)
    grad_q = grad_q + reach_ahead * jnp.einsum(
        "bthv,bhkv->bthk", grad_wide, state_ahead, precision=HIGHEST
    )
    grad_q = grad_q + reach_behind * jnp.einsum(
        "bthv,bhkv->bthk", grad_wide, state_behind, precision=HIGHEST
    )
    grad_k_ahead = jnp.einsum(
        "bhts,bthk->bshk", grad_scores * mask_ahead[None], query_wide, precision=HIGHEST
    )
    grad_k_ahead = grad_k_ahead + keep_ahead * jnp.einsum(
        "bshv,bhkv->bshk", value_wide, pull_ahead, precision=HIGHEST
    )
    grad_k_behind = jnp.einsum(
        "bhts,bthk->bshk", grad_scores * mask_behind[None], query_wide, precision=HIGHEST
    )
    grad_k_behind = grad_k_behind + keep_behind * jnp.einsum(
        "bshv,bhkv->bshk", value_wide, pull_behind, precision=HIGHEST
    )
    grad_v = jnp.einsum("bhts,bthv->bshv", scores * mask_both, grad_wide, precision=HIGHEST)
    grad_v = grad_v + keep_ahead * jnp.einsum(
        "bshk,bhkv->bshv", keys, pull_ahead, precision=HIGHEST
    )
    grad_v = grad_v + keep_behind * jnp.einsum(
        "bshk,bhkv->bshv", keys, pull_behind, precision=HIGHEST
    )
    positions = (my_index * length + offsets)[None, :, None]
    out_dot_ahead = jnp.sum(positions * jnp.sum(out_ahead * grad_wide, axis=3), axis=(0, 1))
    key_dot_ahead = jnp.sum(positions * jnp.sum(keys * grad_k_ahead, axis=3), axis=(0, 1))
    out_dot_behind = jnp.sum(positions * jnp.sum(out_behind * grad_wide, axis=3), axis=(0, 1))
    key_dot_behind = jnp.sum(positions * jnp.sum(keys * grad_k_behind, axis=3), axis=(0, 1))
    local_sums = jnp.stack([out_dot_ahead - key_dot_ahead, key_dot_behind - out_dot_behind])
    rate_sums = lax.psum(local_sums, "sp")
    slopes = jnp.stack([jax.nn.sigmoid(-decay_ahead), jax.nn.sigmoid(-decay_behind)]) / all_tokens
    decay_grad = rate_sums * slopes
    key_grad_raw = ((grad_k_ahead + grad_k_behind) * key_scale).astype(jnp.bfloat16)

    def weight_rows(start, row_count):
        piece = lax.dynamic_slice_in_dim(inputs, start, row_count, 2)
        return jnp.einsum("bld,blhk->dhk", piece, key_grad_raw, preferred_element_type=jnp.float32)

    weight_grad = own_rows(weight_rows, in_width // devices, "sp")

    def input_rows(start, row_count):
        piece = lax.dynamic_slice_in_dim(key_grad_raw, start, row_count, 0)
        return jnp.einsum("blhk,dhk->bld", piece, key_weight, preferred_element_type=jnp.float32)

    input_grad = summed_rows(input_rows, batch_seqs // lax.axis_size("tp"), "tp").astype(
        jnp.bfloat16
    )
    return (
        grad_q.astype(jnp.bfloat16),
        grad_v.astype(jnp.bfloat16),
        input_grad,
        weight_grad,
        decay_grad,
    )


def solution(mesh):
    in_specs = (
        P(None, "sp", None),
        P(None, "sp", "tp", None),
        P(None, "sp", "tp", None),
        P(None, "sp", "tp", None),
        P(None, "tp", None),
        P("tp"),
        P("tp"),
    )
    out_specs = (
        P(None, "sp", "tp", None),
        P(None, "sp", "tp", None),
        P("tp", "sp", None),
        P("sp", "tp", None),
        P(None, "tp"),
    )
    return jax.shard_map(shards, mesh=mesh, in_specs=in_specs, out_specs=out_specs, check_vma=False)
```

profile of v0, /device:TPU:0, one launch (start us, length us, event | category | flops | bytes accessed | tf_op | source)
XLA Modules:
  0.0 462.7 jit_solution(7390019577858132643)
XLA Ops:
  7.3 1.4 copy.106
  8.7 1.3 broadcast_multiply_fusion.3
  10.9 2.1 fusion.41
  14.8 2.1 fusion.37
  17.1 2.1 fusion.40
  19.2 2.1 fusion.36
  21.5 1.3 fusion.92
  23.7 36.6 %all-reduce.3 = (f32[32]{0:T(128)S(1)}, f32[32]{0:T(128)S(1)}) all-reduce(f32[32]{0:T(128)S(1)} %exponential_dynamic-update-slice_fusion, f32[32]{0:T(128)S(1)} %exponential_dynamic-update-slice_fusion.1), channel_id=4, replica_groups=mesh['sp'=16,'tp'=2] {'sp'}, use_global_device_ids=true, to_apply=%add.1 | all-reduce | flops 64 | bytes 512
  61.8 1.6 broadcast_multiply_fusion
  63.4 1.7 copy.122
  65.1 1.7 copy.144
  70.5 19.9 %all-gather.15.cloned.1.call-done = f32[32,2,128,256]{3,2,1,0:T(8,128)} async-done(((f32[2,2,128,256]{3,2,1,0:T(8,128)}), f32[32,2,128,256]{3,2,1,0:T(8,128)}) %all-gather.15.cloned.1.call-update) | async-done | bytes 8388624 | tf_op jit(solution)/shard_map/all_gather | solution.py:12
  90.5 7.6 %rev.13 = f32[16,2,2,128,256]{4,3,2,1,0:T(8,128)} reverse(f32[16,2,2,128,256]{4,3,2,1,0:T(8,128)} %bitcast.160), dimensions={0} | reverse | bytes 16777216 | tf_op jit(solution)/shard_map/rev | solution.py:14
  98.1 67.5 %all-gather.17.cloned.1.call-done = f32[32,2,128,256]{3,2,1,0:T(8,128)} async-done(((f32[2,2,128,256]{3,2,1,0:T(8,128)}), f32[32,2,128,256]{3,2,1,0:T(8,128)}) %all-gather.17.cloned.1.call-update) | async-done | bytes 8388624 | tf_op jit(solution)/shard_map/all_gather | solution.py:12
  165.6 7.6 %rev.15 = f32[16,2,2,128,256]{4,3,2,1,0:T(8,128)} reverse(f32[16,2,2,128,256]{4,3,2,1,0:T(8,128)} %bitcast.161), dimensions={0} | reverse | bytes 16777216 | tf_op jit(solution)/shard_map/rev | solution.py:14
  173.1 42.3 %while.33 = (s32[]{:T(128)}, f32[2,2,128,256]{3,2,1,0:T(8,128)S(1)}, f32[2,2,128,256]{3,2,1,0:T(8,128)S(1)}, s32[]{:T(128)}, f32[16,1,2,1,1]{2,4,3,1,0:T(1,128)}...) while((s32[]{:T(128)}, ...), condition=%wide.region_3.4_spmd.clone, body=%wide.region_2.3_spmd.clone.sunk | while | flops 1048580 | bytes 3145917 | solution.py:24
  174.4 1.5 fusion.118
  177.2 1.5 fusion.118
  180.0 1.5 fusion.118
  182.7 1.5 fusion.118
  185.5 1.5 fusion.118
  188.3 1.5 fusion.118
  191.1 1.5 fusion.118
  193.9 1.5 fusion.118
  196.8 1.5 fusion.118
  199.5 1.8 fusion.118
  202.6 1.5 fusion.118
  205.4 1.5 fusion.118
  208.2 1.5 fusion.118
  211.1 1.5 fusion.118
  213.9 1.5 fusion.118
  216.5 1.4 convolution_bitcast_fusion.2
  218.0 22.7 %all-gather.11.cloned.1.call-done = f32[32,2,128,256]{3,2,1,0:T(8,128)} async-done(((f32[2,2,128,256]{3,2,1,0:T(8,128)}), f32[32,2,128,256]{3,2,1,0:T(8,128)}) %all-gather.11.cloned.1.call-update) | async-done | bytes 8388624 | tf_op jit(solution)/shard_map/all_gather | solution.py:12
  240.6 74.9 %all-gather.13.cloned.1.call-done = f32[32,2,128,256]{3,2,1,0:T(8,128)} async-done(((f32[2,2,128,256]{3,2,1,0:T(8,128)}), f32[32,2,128,256]{3,2,1,0:T(8,128)}) %all-gather.13.cloned.1.call-update) | async-done | bytes 8388624 | tf_op jit(solution)/shard_map/all_gather | solution.py:12
  315.6 23.2 %while.32 = (s32[]{:T(128)}, f32[2,2,128,256]{3,2,1,0:T(8,128)S(1)}, f32[2,2,128,256]{3,2,1,0:T(8,128)S(1)}, s32[]{:T(128)}, f32[16,1,2,1,1]{2,4,3,1,0:T(1,128)S...) while((s32[]{:T(128)}, ...), condition=%wide.region_1.2_spmd.clone, body=%wide.region_0.1_spmd.clone.sunk | while | flops 1048580 | bytes 3145917 | solution.py:24
  315.6 1.5 fusion.115
  317.2 1.5 fusion.115
  318.7 1.5 fusion.115
  320.3 1.5 fusion.115
  321.8 1.5 fusion.115
  323.3 1.5 fusion.115
  324.9 1.5 fusion.115
  326.4 1.5 fusion.115
  328.0 1.5 fusion.115
  329.5 1.5 fusion.115
  331.1 1.5 fusion.115
  332.6 1.5 fusion.115
  334.2 1.5 fusion.115
  335.7 1.5 fusion.115
  337.2 1.5 fusion.115
  338.8 1.1 fusion.20
  341.3 1.8 fusion.38
  343.1 1.3 convolution_bitcast_fusion
  344.4 2.2 copy.136
  347.4 1.6 fusion.18
  349.0 1.4 fusion.19
  351.7 31.6 %psum.7 = f32[2,2]{1,0:T(2,128)S(1)} all-reduce(f32[2,2]{1,0:T(2,128)S(1)} %pad_maximum_fusion), channel_id=1, replica_groups=mesh['sp'=16,'tp'=2] {'sp'}, use_global_device_ids=true, to_apply=%region_14.15 | all-reduce | flops 4 | bytes 32 | tf_op jit(solution)/shard_map/psum | solution.py:154
  383.3 1.7 fusion.28
  385.8 2.2 fusion.8
  389.3 1.3 fusion.17
  391.5 1.3 fusion.83
  392.8 46.6 %all-reduce.6.cloned.1.call-done = f32[1024,2,128]{2,1,0:T(2,128)} async-done(((f32[1024,2,128]{2,1,0:T(2,128)}), f32[1024,2,128]{2,1,0:T(2,128)}) %all-reduce.6.cloned.1.call-update) | async-done | bytes 1048592
  439.4 1.5 constant_dynamic-slice_fusion.4
  440.9 15.0 %reduce-scatter.2.cloned.1.call-done = bf16[1,128,1024]{2,1,0:T(8,128)(2,1)} async-done(((bf16[2,128,1024]{2,1,0:T(8,128)(2,1)}), bf16[1,128,1024]{2,1,0:T(8,128)(2,1)}) %reduce-scatter.2.cloned.1.call-update) | async-done | bytes 262160 | tf_op jit(solution)/shard_map/reduce_scatter | solution.py:34
  (137 shorter events, 34.8 us)
Async XLA Ops:
  7.2 2.8 copy-start
  7.2 62.4 %copy-start.2 = (bf16[2,128,2,256]{3,2,1,0:T(2,128)(2,1)S(1)}, bf16[2,128,2,256]{3,2,1,0:T(2,128)(2,1)}, u32[]{:S(2)}) copy-start(bf16[2,128,2,256]{3,2,1,0:T(2,128)(2,1)} %param.13) | copy-start | bytes 786436
  7.2 62.4 %copy-start.1 = (bf16[2,128,2,256]{3,2,1,0:T(2,128)(2,1)S(1)}, bf16[2,128,2,256]{3,2,1,0:T(2,128)(2,1)}, u32[]{:S(2)}) copy-start(bf16[2,128,2,256]{3,2,1,0:T(2,128)(2,1)} %param.14) | copy-start | bytes 786436
  7.2 83.3 %all-gather.15.cloned.1.call-start = ((), (), s32[]{:S(2)}) async-start(), calls=%async_computation.4 | async-start | bytes 8912896 | tf_op jit(solution)/shard_map/all_gather | solution.py:12
  9.9 11.6 %copy-start.12 = (f32[2]{0:T(128)}, f32[2]{0:T(128)S(1)}, u32[]{:S(2)}) copy-start(f32[2]{0:T(128)S(1)} %get-tuple-element.478) | copy-start | bytes 28
  9.9 11.6 %copy-start.13 = (f32[2]{0:T(128)}, f32[2]{0:T(128)S(1)}, u32[]{:S(2)}) copy-start(f32[2]{0:T(128)S(1)} %get-tuple-element.450) | copy-start | bytes 28
  10.9 10.5 %copy-start.8 = (f32[128,2]{0,1:T(2,128)}, f32[128,2]{0,1:T(2,128)S(1)}, u32[]{:S(2)}) copy-start(f32[128,2]{0,1:T(2,128)S(1)} %get-tuple-element.470) | copy-start | bytes 3076
  13.1 152.5 %all-gather.17.cloned.1.call-start = ((), (), s32[]{:S(2)}) async-start(), calls=%async_computation.5 | async-start | bytes 8912896 | tf_op jit(solution)/shard_map/all_gather | solution.py:12
  14.8 6.6 %copy-start.6 = (f32[128,2]{0,1:T(2,128)}, f32[128,2]{0,1:T(2,128)S(1)}, u32[]{:S(2)}) copy-start(f32[128,2]{0,1:T(2,128)S(1)} %get-tuple-element.467) | copy-start | bytes 3076
  17.0 223.6 %all-gather.11.cloned.1.call-start = ((), (), s32[]{:S(2)}) async-start(), calls=%async_computation.2 | async-start | bytes 8912896 | tf_op jit(solution)/shard_map/all_gather | solution.py:12
  19.2 296.4 %all-gather.13.cloned.1.call-start = ((), (), s32[]{:S(2)}) async-start(), calls=%async_computation.3 | async-start | bytes 8912896 | tf_op jit(solution)/shard_map/all_gather | solution.py:12
  21.4 418.0 %all-reduce.6.cloned.1.call-start = ((), (), s32[]{:S(2)}) async-start(), calls=%async_computation.6 | async-start | bytes 2097152
  173.1 42.3 %copy-start.9 = (f32[128,2]{0,1:T(2,128)S(1)}, f32[128,2]{0,1:T(2,128)}, u32[]{:S(2)}) copy-start(f32[128,2]{0,1:T(2,128)} %copy-done.8) | copy-start | bytes 3076
  315.6 25.4 %copy-start.3 = (f32[2,2,128,128]{3,2,1,0:T(8,128)S(1)}, f32[2,2,128,128]{3,2,1,0:T(8,128)}, u32[]{:S(2)}) copy-start(f32[2,2,128,128]{3,2,1,0:T(8,128)} %fusion.72) | copy-start | bytes 786436
  315.6 25.4 %copy-start.5 = (f32[2,128,128]{2,1,0:T(8,128)S(1)}, f32[2,128,128]{2,1,0:T(8,128)}, u32[]{:S(2)}) copy-start(f32[2,128,128]{2,1,0:T(8,128)} %get-tuple-element.459) | copy-start | bytes 393220
  338.7 8.0 %copy-start.7 = (f32[128,2]{0,1:T(2,128)S(1)}, f32[128,2]{0,1:T(2,128)}, u32[]{:S(2)}) copy-start(f32[128,2]{0,1:T(2,128)} %copy-done.6) | copy-start | bytes 3076
  338.8 8.6 %copy-start.4 = (f32[2,2,128,128]{2,3,1,0:T(8,128)S(1)}, f32[2,2,128,128]{2,3,1,0:T(8,128)}, u32[]{:S(2)}) copy-start(f32[2,2,128,128]{2,3,1,0:T(8,128)} %convolution_bitcast_fusion.16) | copy-start | bytes 786436
  339.9 48.1 %copy-start.10 = (f32[128,2]{0,1:T(2,128)S(1)}, f32[128,2]{0,1:T(2,128)}, u32[]{:S(2)}) copy-start(f32[128,2]{0,1:T(2,128)} %get-tuple-element.468) | copy-start | bytes 3076
  340.9 47.7 %copy-start.11 = (f32[128,2]{0,1:T(2,128)S(1)}, f32[128,2]{0,1:T(2,128)}, u32[]{:S(2)}) copy-start(f32[128,2]{0,1:T(2,128)} %get-tuple-element.461) | copy-start | bytes 3076
  346.7 109.2 %reduce-scatter.2.cloned.1.call-start = ((), (), s32[]{:S(2)}) async-start(), calls=%async_computation.1 | async-start | bytes 786432 | tf_op jit(solution)/shard_map/reduce_scatter | solution.py:34
Sparse Core Ops, SparseCore 0:
  13.2 77.2 all-gather.14
  92.6 72.8 all-gather.16
  167.7 72.8 all-gather.10
  242.6 72.8 all-gather.12
  346.8 92.5 all-reduce.5
  442.1 13.7 reduce-scatter.1
where the time goes:
time: 464 us; the launch traced here: 463 us
  waiting for transfers between devices  247 us (53%)
  blocking collectives  68.2 us (15%)
  other arithmetic  51.9 us (11%)
  local copies, waits for them, and re-layouts  49.5 us (11%)
  matrix products  29.3 us (6%)
  between operations  15.8 us (3%)
    all_gather x4, waiting for transfers between devices, prefix(): pieces = jax.tree.map(lambda part: lax.all_gather(part, axis), value)  185 us
    unnamed x7, waiting for transfers between devices  46.7 us
    select_n x30, other arithmetic, step(): jnp.where(position < mine, new, old)  44.9 us
    unnamed x1, blocking collectives  36.6 us
    psum x1, blocking collectives, shards(): rate_sums = lax.psum(local_sums, 'sp')  31.6 us
    rev x4, local copies, waits for them, and re-layouts, prefix(): pieces = jax.tree.map(lambda part: part[::-1], pieces)  16.4 us
    reduce_scatter x1, waiting for transfers between devices, summed_rows(): lax.psum_scatter(everything.astype(jnp.bfloat16), axis, scatter_dimension...  15 us
    mul x30, local copies, waits for them, and re-layouts, link_states(): later[0] * earlier[1] + later[1]  9.94 us
  transfers between devices with their start and end apart: 6, of which 6 were waited for; matrix products, arithmetic and copies ran while one was open for 20% of the time, Pallas kernels for 0%

commit v1 on v0

--- a/solution.py
+++ b/solution.py
@@ -151,7 +151,10 @@
     out_dot_behind = jnp.sum(positions * jnp.sum(out_behind * grad_wide, axis=3), axis=(0, 1))
     key_dot_behind = jnp.sum(positions * jnp.sum(keys * grad_k_behind, axis=3), axis=(0, 1))
     local_sums = jnp.stack([out_dot_ahead - key_dot_ahead, key_dot_behind - out_dot_behind])
-    rate_sums = lax.psum(local_sums, "sp")
+    count_2, rate_sums = (lax.axis_size("sp"), local_sums)
+    for far in [1 << k for k in range(count_2.bit_length() - 1)]:
+        pairs = [(i, i ^ far) for i in range(count_2)]
+        rate_sums = rate_sums + lax.ppermute(rate_sums, "sp", pairs)
     slopes = jnp.stack([jax.nn.sigmoid(-decay_ahead), jax.nn.sigmoid(-decay_behind)]) / all_tokens
     decay_grad = rate_sums * slopes
     key_grad_raw = ((grad_k_ahead + grad_k_behind) * key_scale).astype(jnp.bfloat16)

time: 464 us -> 495 us (1.067)
  waiting for transfers between devices: 247 us -> 303 us
  blocking collectives: 68.2 us -> 36.6 us
    psum x1 -> x0, blocking collectives: 31.6 us -> none  [shards(): rate_sums = lax.psum(local_sums, 'sp')]
    all_gather x4, waiting for transfers between devices: 185 us -> 212 us  [prefix(): pieces = jax.tree.map(lambda part: lax.all_gather(part, axis), value)]
    unnamed x7, waiting for transfers between devices: 46.7 us -> 67.5 us
    ppermute x0 -> x4, waiting for transfers between devices: none -> 8.89 us  [shards(): rate_sums = rate_sums + lax.ppermute(rate_sums, 'sp', pairs)]
  transfers between devices with their start and end apart: 6 -> 10, of which waited for: 6 -> 10; matrix products, arithmetic and copies ran while one was open for 20% -> 13% of each run, Pallas kernels for 0% -> 0%
where the time goes in v1:
time: 495 us; the launch traced here: 493 us
  waiting for transfers between devices  303 us (61%)
  other arithmetic  51.5 us (10%)
  local copies, waits for them, and re-layouts  50.7 us (10%)
  blocking collectives  36.6 us (7%)
  matrix products  30.4 us (6%)
  between operations  15.8 us (3%)
    all_gather x4, waiting for transfers between devices, prefix(): pieces = jax.tree.map(lambda part: lax.all_gather(part, axis), value)  212 us
    unnamed x7, waiting for transfers between devices  67.5 us
    select_n x30, other arithmetic, step(): jnp.where(position < mine, new, old)  44.5 us
    unnamed x1, blocking collectives  36.6 us
    rev x4, local copies, waits for them, and re-layouts, prefix(): pieces = jax.tree.map(lambda part: part[::-1], pieces)  16.4 us
    reduce_scatter x1, waiting for transfers between devices, summed_rows(): lax.psum_scatter(everything.astype(jnp.bfloat16), axis, scatter_dimension...  15 us
    mul x30, local copies, waits for them, and re-layouts, link_states(): later[0] * earlier[1] + later[1]  9.93 us
  transfers between devices with their start and end apart: 10, of which 10 were waited for; matrix products, arithmetic and copies ran while one was open for 13% of the time, Pallas kernels for 0%

profile of v1, /device:TPU:0, one launch (start us, length us, event | category | flops | bytes accessed | tf_op | source)
XLA Modules:
  0.0 493.5 jit_solution(2948486079307827320)
XLA Ops:
  7.3 1.4 copy.106
  10.9 2.2 fusion.41
  13.8 2.1 fusion.40
  17.1 2.1 fusion.36
  19.3 2.1 fusion.37
  21.5 1.4 fusion.93
  23.8 36.6 %all-reduce.3 = (f32[32]{0:T(128)S(1)}, f32[32]{0:T(128)S(1)}) all-reduce(f32[32]{0:T(128)S(1)} %exponential_dynamic-update-slice_fusion, f32[32]{0:T(128)S(1)} %exponential_dynamic-update-slice_fusion.1), channel_id=4, replica_groups=mesh['sp'=16,'tp'=2] {'sp'}, use_global_device_ids=true, to_apply=%add.1 | all-reduce | flops 64 | bytes 512
  61.9 1.6 broadcast_multiply_fusion
  63.5 1.6 copy.122
  65.1 1.6 copy.144
  70.5 20.0 %all-gather.15.cloned.1.call-done = f32[32,2,128,256]{3,2,1,0:T(8,128)} async-done(((f32[2,2,128,256]{3,2,1,0:T(8,128)}), f32[32,2,128,256]{3,2,1,0:T(8,128)}) %all-gather.15.cloned.1.call-update) | async-done | bytes 8388624 | tf_op jit(solution)/shard_map/all_gather | solution.py:12
  90.5 7.6 %rev.13 = f32[16,2,2,128,256]{4,3,2,1,0:T(8,128)} reverse(f32[16,2,2,128,256]{4,3,2,1,0:T(8,128)} %bitcast.161), dimensions={0} | reverse | bytes 16777216 | tf_op jit(solution)/shard_map/rev | solution.py:14
  98.1 67.5 %all-gather.11.cloned.1.call-done = f32[32,2,128,256]{3,2,1,0:T(8,128)} async-done(((f32[2,2,128,256]{3,2,1,0:T(8,128)}), f32[32,2,128,256]{3,2,1,0:T(8,128)}) %all-gather.11.cloned.1.call-update) | async-done | bytes 8388624 | tf_op jit(solution)/shard_map/all_gather | solution.py:12
  165.6 75.1 %all-gather.13.cloned.1.call-done = f32[32,2,128,256]{3,2,1,0:T(8,128)} async-done(((f32[2,2,128,256]{3,2,1,0:T(8,128)}), f32[32,2,128,256]{3,2,1,0:T(8,128)}) %all-gather.13.cloned.1.call-update) | async-done | bytes 8388624 | tf_op jit(solution)/shard_map/all_gather | solution.py:12
  240.7 23.3 %while.32 = (s32[]{:T(128)}, f32[2,2,128,256]{3,2,1,0:T(8,128)S(1)}, f32[2,2,128,256]{3,2,1,0:T(8,128)S(1)}, s32[]{:T(128)}, f32[16,1,2,1,1]{2,4,3,1,0:T(1,128)S...) while((s32[]{:T(128)}, ...), condition=%wide.region_1.2_spmd.clone, body=%wide.region_0.1_spmd.clone.sunk | while | flops 1048580 | bytes 3145917 | solution.py:24
  240.7 1.5 fusion.117
  242.2 1.5 fusion.117
  243.7 1.5 fusion.117
  245.3 1.5 fusion.117
  246.8 1.5 fusion.117
  248.4 1.6 fusion.117
  250.0 1.5 fusion.117
  251.6 1.5 fusion.117
  253.1 1.5 fusion.117
  254.7 1.5 fusion.117
  256.2 1.5 fusion.117
  257.8 1.5 fusion.117
  259.3 1.5 fusion.117
  260.9 1.5 fusion.117
  262.4 1.5 fusion.117
  265.0 1.4 fusion.16
  266.5 49.1 %all-gather.17.cloned.1.call-done = f32[32,2,128,256]{3,2,1,0:T(8,128)} async-done(((f32[2,2,128,256]{3,2,1,0:T(8,128)}), f32[32,2,128,256]{3,2,1,0:T(8,128)}) %all-gather.17.cloned.1.call-update) | async-done | bytes 8388624 | tf_op jit(solution)/shard_map/all_gather | solution.py:12
  315.6 7.6 %rev.15 = f32[16,2,2,128,256]{4,3,2,1,0:T(8,128)} reverse(f32[16,2,2,128,256]{4,3,2,1,0:T(8,128)} %bitcast.160), dimensions={0} | reverse | bytes 16777216 | tf_op jit(solution)/shard_map/rev | solution.py:14
  323.2 42.0 %while.33 = (s32[]{:T(128)}, f32[2,2,128,256]{3,2,1,0:T(8,128)S(1)}, f32[2,2,128,256]{3,2,1,0:T(8,128)S(1)}, s32[]{:T(128)}, f32[16,1,2,1,1]{2,4,3,1,0:T(1,128)}...) while((s32[]{:T(128)}, ...), condition=%wide.region_3.4_spmd.clone, body=%wide.region_2.3_spmd.clone.sunk | while | flops 1048580 | bytes 3145917 | solution.py:24
  324.6 1.5 fusion.120
  327.4 1.5 fusion.120
  330.2 1.5 fusion.120
  333.0 1.5 fusion.120
  335.8 1.5 fusion.120
  338.6 1.5 fusion.120
  341.4 1.5 fusion.120
  344.2 1.5 fusion.120
  347.0 1.5 fusion.120
  349.8 1.5 fusion.120
  352.5 1.5 fusion.120
  355.3 1.5 fusion.120
  358.1 1.5 fusion.120
  360.9 1.5 fusion.120
  363.8 1.5 fusion.120
  365.3 1.4 fusion.15
  369.7 2.2 fusion.8
  375.3 2.2 copy.136
  377.9 2.2 fusion.17
  380.1 1.7 fusion.28
  382.6 1.9 copy.151
  385.8 1.4 fusion.18
  390.4 3.0 collective-permute-done.1
  393.4 1.3 collective-permute-start.2
  394.7 2.3 collective-permute-done.2
  397.1 1.8 collective-permute-start.3
  398.9 2.6 collective-permute-done.3
  402.8 67.4 %all-reduce.6.cloned.1.call-done = f32[1024,2,128]{2,1,0:T(2,128)} async-done(((f32[1024,2,128]{2,1,0:T(2,128)}), f32[1024,2,128]{2,1,0:T(2,128)}) %all-reduce.6.cloned.1.call-update) | async-done | bytes 1048592
  470.2 1.5 constant_dynamic-slice_fusion.4
  471.7 15.0 %reduce-scatter.2.cloned.1.call-done = bf16[1,128,1024]{2,1,0:T(8,128)(2,1)} async-done(((bf16[2,128,1024]{2,1,0:T(8,128)(2,1)}), bf16[1,128,1024]{2,1,0:T(8,128)(2,1)}) %reduce-scatter.2.cloned.1.call-update) | async-done | bytes 262160 | tf_op jit(solution)/shard_map/reduce_scatter | solution.py:34
  (151 shorter events, 43.0 us)
Async XLA Ops:
  7.2 2.8 copy-start
  7.2 62.4 %copy-start.2 = (bf16[2,128,2,256]{3,2,1,0:T(2,128)(2,1)S(1)}, bf16[2,128,2,256]{3,2,1,0:T(2,128)(2,1)}, u32[]{:S(2)}) copy-start(bf16[2,128,2,256]{3,2,1,0:T(2,128)(2,1)} %param.13) | copy-start | bytes 786436
  7.2 62.4 %copy-start.1 = (bf16[2,128,2,256]{3,2,1,0:T(2,128)(2,1)S(1)}, bf16[2,128,2,256]{3,2,1,0:T(2,128)(2,1)}, u32[]{:S(2)}) copy-start(bf16[2,128,2,256]{3,2,1,0:T(2,128)(2,1)} %param.14) | copy-start | bytes 786436
  7.2 83.3 %all-gather.15.cloned.1.call-start = ((), (), s32[]{:S(2)}) async-start(), calls=%async_computation.4 | async-start | bytes 8912896 | tf_op jit(solution)/shard_map/all_gather | solution.py:12
  9.9 11.6 %copy-start.14 = (f32[2]{0:T(128)}, f32[2]{0:T(128)S(1)}, u32[]{:S(2)}) copy-start(f32[2]{0:T(128)S(1)} %get-tuple-element.478) | copy-start | bytes 28
  9.9 11.6 %copy-start.15 = (f32[2]{0:T(128)}, f32[2]{0:T(128)S(1)}, u32[]{:S(2)}) copy-start(f32[2]{0:T(128)S(1)} %get-tuple-element.450) | copy-start | bytes 28
  10.9 10.5 %copy-start.8 = (f32[128,2]{0,1:T(2,128)}, f32[128,2]{0,1:T(2,128)S(1)}, u32[]{:S(2)}) copy-start(f32[128,2]{0,1:T(2,128)S(1)} %get-tuple-element.470) | copy-start | bytes 3076
  13.1 152.5 %all-gather.11.cloned.1.call-start = ((), (), s32[]{:S(2)}) async-start(), calls=%async_computation.2 | async-start | bytes 8912896 | tf_op jit(solution)/shard_map/all_gather | solution.py:12
  13.8 7.6 %copy-start.10 = (f32[128,2]{0,1:T(2,128)}, f32[128,2]{0,1:T(2,128)S(1)}, u32[]{:S(2)}) copy-start(f32[128,2]{0,1:T(2,128)S(1)} %get-tuple-element.467) | copy-start | bytes 3076
  16.0 224.7 %all-gather.13.cloned.1.call-start = ((), (), s32[]{:S(2)}) async-start(), calls=%async_computation.3 | async-start | bytes 8912896 | tf_op jit(solution)/shard_map/all_gather | solution.py:12
  19.2 296.4 %all-gather.17.cloned.1.call-start = ((), (), s32[]{:S(2)}) async-start(), calls=%async_computation.5 | async-start | bytes 8912896 | tf_op jit(solution)/shard_map/all_gather | solution.py:12
  21.4 448.8 %all-reduce.6.cloned.1.call-start = ((), (), s32[]{:S(2)}) async-start(), calls=%async_computation.6 | async-start | bytes 2097152
  98.1 165.8 %copy-start.13 = (f32[128,2]{0,1:T(2,128)S(1)}, f32[128,2]{0,1:T(2,128)}, u32[]{:S(2)}) copy-start(f32[128,2]{0,1:T(2,128)} %get-tuple-element.468) | copy-start | bytes 3076
  323.2 42.1 %copy-start.12 = (f32[128,2]{0,1:T(2,128)S(1)}, f32[128,2]{0,1:T(2,128)}, u32[]{:S(2)}) copy-start(f32[128,2]{0,1:T(2,128)} %get-tuple-element.461) | copy-start | bytes 3076
  323.2 43.9 %copy-start.3 = (f32[2,2,128,128]{3,2,1,0:T(8,128)S(1)}, f32[2,2,128,128]{3,2,1,0:T(8,128)}, u32[]{:S(2)}) copy-start(f32[2,2,128,128]{3,2,1,0:T(8,128)} %fusion.72) | copy-start | bytes 786436
  323.2 43.9 %copy-start.7 = (f32[2,128,128]{2,1,0:T(8,128)S(1)}, f32[2,128,128]{2,1,0:T(8,128)}, u32[]{:S(2)}) copy-start(f32[2,128,128]{2,1,0:T(8,128)} %get-tuple-element.459) | copy-start | bytes 393220
  323.2 50.0 %copy-start.9 = (f32[128,2]{0,1:T(2,128)S(1)}, f32[128,2]{0,1:T(2,128)}, u32[]{:S(2)}) copy-start(f32[128,2]{0,1:T(2,128)} %copy-done.8) | copy-start | bytes 3076
  323.2 51.0 %copy-start.11 = (f32[128,2]{0,1:T(2,128)S(1)}, f32[128,2]{0,1:T(2,128)}, u32[]{:S(2)}) copy-start(f32[128,2]{0,1:T(2,128)} %copy-done.10) | copy-start | bytes 3076
  365.3 12.6 %copy-start.4 = (f32[2,2,128,128]{2,3,1,0:T(8,128)S(1)}, f32[2,2,128,128]{2,3,1,0:T(8,128)}, u32[]{:S(2)}) copy-start(f32[2,2,128,128]{2,3,1,0:T(8,128)} %convolution_bitcast_fusion.16) | copy-start | bytes 786436
  367.1 10.8 %copy-start.5 = (f32[2,128,2,256]{3,1,2,0:T(8,128)S(1)}, f32[2,128,2,256]{3,1,2,0:T(8,128)}, u32[]{:S(2)}) copy-start(f32[2,128,2,256]{3,1,2,0:T(8,128)} %fusion.16) | copy-start | bytes 1572868
  373.2 14.1 %copy-start.6 = (f32[2,128,128]{1,2,0:T(8,128)S(1)}, f32[2,128,128]{1,2,0:T(8,128)}, u32[]{:S(2)}) copy-start(f32[2,128,128]{1,2,0:T(8,128)} %copy.137) | copy-start | bytes 393220
  377.6 109.0 %reduce-scatter.2.cloned.1.call-start = ((), (), s32[]{:S(2)}) async-start(), calls=%async_computation.1 | async-start | bytes 786432 | tf_op jit(solution)/shard_map/reduce_scatter | solution.py:34
  388.6 1.2 collective-permute-start
  389.8 3.6 collective-permute-start.1
  393.4 3.6 collective-permute-start.2
  397.1 4.5 collective-permute-start.3
Sparse Core Ops, SparseCore 0:
  13.2 77.2 all-gather.14
  92.7 72.8 all-gather.10
  167.7 72.8 all-gather.12
  242.7 72.8 all-gather.16
  377.7 92.3 all-reduce.5
  472.9 13.7 reduce-scatter.1
